TPU v7x, 512 devices: a 4x2x32 block of a 4x8x32 slice. The times are simulated.
512 devices in a mesh: grp: 2 (over y), tp: 32 (over z), dp: 8 (over x, core).
Axes of the slice: x: 4, y: 2, z: 32, core: 2. Of those that a mesh axis runs over, the one named last changes fastest.
The devices are a block of a 4x8x32 slice.
Arguments:
- hidden_in: bfloat16 [192, 4096], P(('grp', 'tp'), 'dp'), parts along dimension 0, may hold values from -40 to 40
- input_norm_gain: float32 [2, 4096], P(None, 'dp'), may hold values from 0.1 to 1.9
- w_query: bfloat16 [2, 4096, 2048], P(None, 'dp', 'tp'), may hold values from -0.09375 to 0.09375
- w_key: bfloat16 [2, 4096, 2048], P(None, 'dp', 'tp'), may hold values from -0.09375 to 0.09375
- w_decay: bfloat16 [2, 4096, 2048], P(None, 'dp', 'tp'), may hold values from -0.375 to 0.375
- w_value: bfloat16 [2, 4096, 4096], P(None, 'dp', 'tp'), may hold values from -0.09375 to 0.09375
- w_gate: bfloat16 [2, 4096, 4096], P(None, 'dp', 'tp'), may hold values from -0.09375 to 0.09375
- out_gain: float32 [2, 4096], P(None, 'tp'), may hold values from 0.1 to 1.9
- w_out: bfloat16 [2, 4096, 4096], P(None, 'tp', 'dp'), may hold values from -0.09375 to 0.09375
- decay_offset: float32 [2, 192, 2048], P(None, ('grp', 'dp'), 'tp'), parts along dimension 1, may hold values from -0.7 to 0
- state: float32 [2, 192, 32, 64, 128], P(None, ('grp', 'dp'), 'tp'), parts along dimension 1, may hold values from -3 to 3
Outputs:
- hidden_out: bfloat16 [192, 4096], P(('grp', 'tp'), 'dp'), parts along dimension 0
- new_state: float32 [2, 192, 32, 64, 128], P(None, ('grp', 'dp'), 'tp'), parts along dimension 1
There are 2 independent parts, one for each index of `grp`. A program takes and returns all parts, laid end to end along the dimension named above; an argument that names none is the same for every part. Nothing has to cross between parts.
All inputs are finite; a program needn't handle non-finite values.
Results may differ from a plain program's by a relative error of at most 0.017.
Values may be sent and summed in bfloat16 or wider, within the bound.
No kernel may reach another device: no remote copies, remote signals or barrier semaphores. Data moves between devices by JAX's collectives and lax.ppermute only.
A program may use at most 64 MiB of HBM per device.

v0:
```python
import jax
import jax.numpy as jnp
from jax import lax
from jax.sharding import Mesh, PartitionSpec as P


D = 4096
HEAD_KEY = 64
VALUE_CHANNELS = 128
LAYERS = 2
LANES = 128
NEAR = 4


epsilon = 1e-06
softness_factor = 16.0

TP = ("far", "near")


def size_of(axes):
    return lax.psum(1, axes)


def exchange(blocks, axes):
    return lax.all_to_all(blocks, axes, split_axis=0, concat_axis=0, tiled=True)


def copies(value, axes):
    return exchange(jnp.broadcast_to(value[None], (size_of(axes), *value.shape)), axes)


def summed(blocks):
    return blocks.astype(jnp.float32).sum(axis=0)


def two_terms(value):
    high = lax.reduce_precision(value, 8, 7)
    return high.astype(jnp.bfloat16), (value - high).astype(jnp.bfloat16)


def per_device(
    hidden_in,
    input_norm_gain,
    w_query,
    w_key,
    w_decay,
    w_value,
    w_gate,
    out_gain,
    w_out,
    decay_offset,
    state,
):
    seq_rows = state.shape[1]
    local_heads = state.shape[2]
    key_cols = local_heads * HEAD_KEY
    value_cols = local_heads * VALUE_CHANNELS
    own_rows, features = hidden_in.shape
    n_dp = size_of("dp")
    n_near = size_of("near")
    hidden = lax.optimization_barrier(copies(hidden_in, TP).reshape(-1, features))
    joined = lax.optimization_barrier(
        [
            jnp.concatenate(
                [m[i] for m in (w_value, w_gate, w_query, w_key, w_decay)], axis=1
            )
            for i in range(LAYERS)
        ]
    )
    gains, offsets = lax.optimization_barrier(
        (
            [out_gain[i].reshape(1, local_heads, VALUE_CHANNELS) for i in range(LAYERS)],
            [decay_offset[i] for i in range(LAYERS)],
        )
    )
    batch = hidden.shape[0]
    states = []
    for index_of_block in range(LAYERS):
        widened = hidden.astype(jnp.float32)
        squares = jnp.sum(widened * widened, axis=1, keepdims=True)
        scaled = (widened * input_norm_gain[index_of_block][None, :]).astype(jnp.bfloat16)
        partial_value = jnp.dot(
            scaled, joined[index_of_block], preferred_element_type=jnp.float32
        ).astype(jnp.bfloat16)
        used = partial_value.shape[1]
        spare = -(used + 2) % LANES
        sent = jnp.concatenate(
            [partial_value, *two_terms(squares), jnp.zeros((batch, spare), jnp.bfloat16)], axis=1
        )
        summed_parts = summed(exchange(sent.reshape(n_dp, seq_rows, -1), "dp"))
        own_squares = jnp.sum(summed_parts[:, used : used + 2], axis=1, keepdims=True)
        inverse = lax.rsqrt(own_squares / D + epsilon)
        projected = summed_parts[:, :used] * inverse
        value_rows = projected[:, :value_cols].reshape(seq_rows, local_heads, VALUE_CHANNELS)
        gate_rows = projected[:, value_cols : 2 * value_cols].reshape(
            seq_rows, local_heads, VALUE_CHANNELS
        )
        rest = projected[:, 2 * value_cols :]
        query_rows = rest[:, :key_cols].reshape(seq_rows, local_heads, HEAD_KEY)
        key_rows = rest[:, key_cols : 2 * key_cols].reshape(
            seq_rows, local_heads, HEAD_KEY
        ) * HEAD_KEY ** (-0.5)
        decay_logits = rest[:, 2 * key_cols :]
        decay_logarithm = (
            jax.nn.log_sigmoid(decay_logits) / softness_factor + offsets[index_of_block]
        )
        decay_rate = jnp.exp(decay_logarithm).reshape(seq_rows, local_heads, HEAD_KEY)
        fresh = (
            decay_rate[:, :, :, None] * state[index_of_block]
            + key_rows[:, :, :, None] * value_rows[:, :, None, :]
        )
        states.append(fresh)
        readout = jnp.sum(query_rows[:, :, :, None] * fresh, axis=2)
        normed = readout * lax.rsqrt(jnp.mean(readout * readout, axis=2, keepdims=True) + epsilon)
        normed = normed * gains[index_of_block]
        gated_out = (
            (normed * jax.nn.silu(gate_rows)).reshape(seq_rows, value_cols).astype(jnp.bfloat16)
        )
        head_terms = jnp.dot(
            copies(gated_out, "dp").reshape(batch, value_cols),
            w_out[index_of_block],
            preferred_element_type=jnp.float32,
        )
        head_terms = head_terms + hidden.astype(jnp.float32) * (1.0 / size_of(TP))
        head_terms = head_terms.astype(jnp.bfloat16)
        if index_of_block + 1 == LAYERS:
            blocks = head_terms.reshape(-1, n_near, own_rows, features).swapaxes(0, 1)
            near_sum = summed(exchange(blocks, "near"))
            hidden_out = summed(exchange(near_sum.astype(jnp.bfloat16), "far"))
        else:
            near_sum = summed(exchange(head_terms.reshape(n_near, -1, features), "near"))
            far_sum = summed(copies(near_sum.astype(jnp.bfloat16), "far"))
            hidden = copies(far_sum.astype(jnp.bfloat16), "near").reshape(batch, features)
    return (hidden_out.astype(jnp.bfloat16), jnp.stack(states))


def solution(mesh):
    sizes = mesh.shape
    fine = Mesh(
        mesh.devices.reshape(sizes["grp"], sizes["tp"] // NEAR, NEAR, sizes["dp"]),
        ("grp", *TP, "dp"),
    )

    return jax.shard_map(
        per_device,
        mesh=fine,
        in_specs=(
            P(("grp", *TP), "dp"),
            P(None, "dp"),
            P(None, "dp", TP),
            P(None, "dp", TP),
            P(None, "dp", TP),
            P(None, "dp", TP),
            P(None, "dp", TP),
            P(None, TP),
            P(None, TP, "dp"),
            P(None, ("grp", "dp"), TP),
            P(None, ("grp", "dp"), TP, None, None),
        ),
        out_specs=(P(("grp", *TP), "dp"), P(None, ("grp", "dp"), TP, None, None)),
        check_vma=False,
    )
```

profile of v0, /device:TPU:40, one launch (start us, length us, event | category | flops | bytes accessed | tf_op | source)
XLA Modules:
  0.0 209.2 jit_solution(15558733298426951348)
XLA Ops:
  0.6 1.4 broadcast_in_dim.10
  2.0 45.9 %all-to-all-start = ((bf16[32,3,512]{2,1,0:T(4,128)(2,1)}), bf16[32,3,512]{2,1,0:T(4,128)(2,1)S(1)}, u32[]{:S(2)}, u32[]{:S(2)}) async-start(bf16[32,3,512]{2,1,0:T(4,128)(2,1)} %broadcast_in_dim.10), calls=%async_computation | async-start | bytes 262144 | tf_op jit(solution)/shard_map/all_to_all | solution.py:26
  48.0 0.9 copy-done.2
  49.0 0.9 copy-done.6
  50.6 0.3 concatenate.21
  51.0 0.3 concatenate.20
  51.4 0.3 copy-done.8
  51.7 27.1 %all-to-all-done = bf16[32,3,512]{2,1,0:T(4,128)(2,1)S(1)} async-done(((bf16[32,3,512]{2,1,0:T(4,128)(2,1)}), bf16[32,3,512]{2,1,0:T(4,128)(2,1)S(1)}, u32[]{:S(2)}, u32[]{:S(2)}) %all-to-all-start) | async-done | bytes 98336 | tf_op jit(solution)/shard_map/all_to_all | solution.py:26
  79.0 0.2 convolution_convert_fusion.1
  79.7 0.8 maximum_maximum_fusion
  80.4 4.7 %all-to-all-start.1 = ((bf16[8,12,512]{2,1,0:T(8,128)(2,1)}), bf16[8,12,512]{2,1,0:T(8,128)(2,1)S(1)}, u32[]{:S(2)}, u32[]{:S(2)}) async-start(bf16[8,12,512]{2,1,0:T(8,128)(2,1)} %maximum_maximum_fusion), calls=%async_computation.1 | async-start | bytes 262144 | tf_op jit(solution)/shard_map/all_to_all | solution.py:26
  85.2 6.1 %all-to-all-done.1 = bf16[8,12,512]{2,1,0:T(8,128)(2,1)S(1)} async-done(((bf16[8,12,512]{2,1,0:T(8,128)(2,1)}), bf16[8,12,512]{2,1,0:T(8,128)(2,1)S(1)}, u32[]{:S(2)}, u32[]{:S(2)}) %all-to-all-start.1) | async-done | bytes 98336 | tf_op jit(solution)/shard_map/all_to_all | solution.py:26
  91.3 0.2 slice_reduce_fusion.1
  91.6 0.4 fusion.7
  92.3 7.9 %all_to_all.50 = bf16[8,12,128]{2,1,0:T(8,128)(2,1)S(1)} all-to-all(bf16[8,12,128]{2,1,0:T(8,128)(2,1)S(1)} %broadcast_in_dim.11), channel_id=1, replica_groups=mesh['grp'=2,'far'=8,'near'=4,'dp'=8] {'dp'}, dimensions={0} | all-to-all | bytes 49152 | tf_op jit(solution)/shard_map/all_to_all | solution.py:26
  100.2 0.2 fusion
  100.3 8.3 %all_to_all.51 = bf16[4,24,512]{2,1,0:T(8,128)(2,1)S(1)} all-to-all(bf16[4,24,512]{2,1,0:T(8,128)(2,1)S(1)} %bitcast.67), channel_id=1, replica_groups=mesh['grp'=2,'far'=8,'near'=4,'dp'=8] {'near'}, dimensions={0} | all-to-all | bytes 196608 | tf_op jit(solution)/shard_map/all_to_all | solution.py:26
  108.6 35.4 %all_to_all.52 = bf16[8,24,512]{2,1,0:T(8,128)(2,1)S(1)} all-to-all(bf16[8,24,512]{2,1,0:T(8,128)(2,1)S(1)} %broadcast_in_dim.12), channel_id=1, replica_groups=mesh['grp'=2,'far'=8,'near'=4,'dp'=8] {'far'}, dimensions={0} | all-to-all | bytes 393216 | tf_op jit(solution)/shard_map/all_to_all | solution.py:26
  144.0 9.7 %all_to_all.53 = bf16[4,24,512]{2,1,0:T(8,128)(2,1)S(1)} all-to-all(bf16[4,24,512]{2,1,0:T(8,128)(2,1)S(1)} %broadcast_in_dim.13), channel_id=1, replica_groups=mesh['grp'=2,'far'=8,'near'=4,'dp'=8] {'near'}, dimensions={0} | all-to-all | bytes 196608 | tf_op jit(solution)/shard_map/all_to_all | solution.py:26
  153.8 0.2 convolution_convert_fusion
  154.6 8.6 %all_to_all.54 = bf16[8,12,512]{2,1,0:T(8,128)(2,1)S(1)} all-to-all(bf16[8,12,512]{2,1,0:T(8,128)(2,1)S(1)} %maximum_maximum_fusion.1), channel_id=1, replica_groups=mesh['grp'=2,'far'=8,'near'=4,'dp'=8] {'dp'}, dimensions={0} | all-to-all | bytes 196608 | tf_op jit(solution)/shard_map/all_to_all | solution.py:26
  163.2 0.2 slice_reduce_fusion
  163.5 0.4 fusion.4
  164.2 7.9 %all_to_all.55 = bf16[8,12,128]{2,1,0:T(8,128)(2,1)S(1)} all-to-all(bf16[8,12,128]{2,1,0:T(8,128)(2,1)S(1)} %broadcast_in_dim.14), channel_id=1, replica_groups=mesh['grp'=2,'far'=8,'near'=4,'dp'=8] {'dp'}, dimensions={0} | all-to-all | bytes 49152 | tf_op jit(solution)/shard_map/all_to_all | solution.py:26
  172.1 0.2 fusion.1
  172.4 8.3 %all_to_all.56 = bf16[4,8,3,512]{3,1,2,0:T(8,128)(2,1)S(1)} all-to-all(bf16[4,8,3,512]{3,1,2,0:T(8,128)(2,1)S(1)} %copy.102), channel_id=1, replica_groups=mesh['grp'=2,'far'=8,'near'=4,'dp'=8] {'near'}, dimensions={0} | all-to-all | bytes 196608 | tf_op jit(solution)/shard_map/all_to_all | solution.py:26
  180.7 0.6 copy.103
  181.3 4.7 %all-to-all-start.9 = ((bf16[8,3,512]{2,1,0:T(4,128)(2,1)}), bf16[8,3,512]{2,1,0:T(4,128)(2,1)S(1)}, u32[]{:S(2)}, u32[]{:S(2)}) async-start(bf16[8,3,512]{2,1,0:T(4,128)(2,1)} %copy.103), calls=%async_computation.9 | async-start | bytes 65536 | tf_op jit(solution)/shard_map/all_to_all | solution.py:26
  186.0 0.5 multiply_add_fusion.1
  186.5 0.9 pad_maximum_fusion
  187.4 21.1 %all-to-all-done.9 = bf16[8,3,512]{2,1,0:T(4,128)(2,1)S(1)} async-done(((bf16[8,3,512]{2,1,0:T(4,128)(2,1)}), bf16[8,3,512]{2,1,0:T(4,128)(2,1)S(1)}, u32[]{:S(2)}, u32[]{:S(2)}) %all-to-all-start.9) | async-done | bytes 24608 | tf_op jit(solution)/shard_map/all_to_all | solution.py:26
  208.5 0.6 reduce_sum.157
  (75 shorter events, 3.3 us)
Async XLA Ops:
  2.0 45.9 %copy-start.4 = (bf16[2,512,64]{1,2,0:T(8,128)(2,1)S(1)}, bf16[2,512,64]{1,2,0:T(8,128)(2,1)}, u32[]{:S(2)}) copy-start(bf16[2,512,64]{1,2,0:T(8,128)(2,1)} %param.15) | copy-start | bytes 393220
  2.0 46.0 %copy-start.5 = (bf16[2,512,64]{1,2,0:T(8,128)(2,1)S(1)}, bf16[2,512,64]{1,2,0:T(8,128)(2,1)}, u32[]{:S(2)}) copy-start(bf16[2,512,64]{1,2,0:T(8,128)(2,1)} %param.13) | copy-start | bytes 393220
  2.0 76.8 %all-to-all-start = ((bf16[32,3,512]{2,1,0:T(4,128)(2,1)}), bf16[32,3,512]{2,1,0:T(4,128)(2,1)S(1)}, u32[]{:S(2)}, u32[]{:S(2)}) async-start(bf16[32,3,512]{2,1,0:T(4,128)(2,1)} %broadcast_in_dim.10), calls=%async_computation | async-start | bytes 262144 | tf_op jit(solution)/shard_map/all_to_all | solution.py:26
  47.9 1.0 copy-start.2
  47.9 1.0 copy-start.3
  49.0 0.9 copy-start.6
  50.9 0.7 copy-start.8
  51.0 0.7 copy-start.7
  79.3 12.4 %copy-start = (f32[2,12,1,64,128]{4,3,2,1,0:T(8,128)S(1)}, f32[2,12,1,64,128]{4,3,2,1,0:T(8,128)}, u32[]{:S(2)}) copy-start(f32[2,12,1,64,128]{4,3,2,1,0:T(8,128)} %param.21) | copy-start | bytes 2359300
  80.4 4.7 %copy-start.9 = (f32[2,128]{1,0:T(2,128)S(1)}, f32[2,128]{1,0:T(2,128)}, u32[]{:S(2)}) copy-start(f32[2,128]{1,0:T(2,128)} %param.18) | copy-start | bytes 3076
  80.4 10.8 %all-to-all-start.1 = ((bf16[8,12,512]{2,1,0:T(8,128)(2,1)}), bf16[8,12,512]{2,1,0:T(8,128)(2,1)S(1)}, u32[]{:S(2)}, u32[]{:S(2)}) async-start(bf16[8,12,512]{2,1,0:T(8,128)(2,1)} %maximum_maximum_fusion), calls=%async_computation.1 | async-start | bytes 262144 | tf_op jit(solution)/shard_map/all_to_all | solution.py:26
  91.6 8.5 %copy-start.1 = (bf16[2,128,512]{2,1,0:T(8,128)(2,1)S(1)}, bf16[2,128,512]{2,1,0:T(8,128)(2,1)}, u32[]{:S(2)}) copy-start(bf16[2,128,512]{2,1,0:T(8,128)(2,1)} %param.19) | copy-start | bytes 786436
  181.3 27.3 %all-to-all-start.9 = ((bf16[8,3,512]{2,1,0:T(4,128)(2,1)}), bf16[8,3,512]{2,1,0:T(4,128)(2,1)S(1)}, u32[]{:S(2)}, u32[]{:S(2)}) async-start(bf16[8,3,512]{2,1,0:T(4,128)(2,1)} %copy.103), calls=%async_computation.9 | async-start | bytes 65536 | tf_op jit(solution)/shard_map/all_to_all | solution.py:26
where the time goes:
time: 210 us; the launch traced here: 209 us
  blocking collectives  85.9 us (41%)
  starting transfers between devices  55.3 us (26%)
  waiting for transfers between devices  54.3 us (26%)
  local copies, waits for them, and re-layouts  6.76 us (3%)
  other arithmetic  5.11 us (2%)
    all_to_all x7, blocking collectives, exchange(): return lax.all_to_all(blocks, axes, split_axis=0, concat_axis=0, tiled=True)  85.9 us
    all_to_all x3, starting transfers between devices, exchange(): return lax.all_to_all(blocks, axes, split_axis=0, concat_axis=0, tiled=True)  55.3 us
    all_to_all x3, waiting for transfers between devices, exchange(): return lax.all_to_all(blocks, axes, split_axis=0, concat_axis=0, tiled=True)  54.3 us
  transfers between devices with their start and end apart: 3, of which 3 were waited for; matrix products, arithmetic and copies ran while one was open for 1% of the time, Pallas kernels for 0%

commit v1 on v0

--- a/solution.py
+++ b/solution.py
@@ -15,7 +15,10 @@
 epsilon = 1e-06
 softness_factor = 16.0
 
-TP = ("far", "near")
+HALVES = 2
+
+TP = ("half", "stride", "near")
+FAR = ("stride", "half")
 
 
 def size_of(axes):
@@ -125,12 +128,13 @@
         head_terms = head_terms + hidden.astype(jnp.float32) * (1.0 / size_of(TP))
         head_terms = head_terms.astype(jnp.bfloat16)
         if index_of_block + 1 == LAYERS:
-            blocks = head_terms.reshape(-1, n_near, own_rows, features).swapaxes(0, 1)
+            blocks = head_terms.reshape(HALVES, -1, n_near, own_rows, features)
+            blocks = blocks.transpose(2, 1, 0, 3, 4).reshape(n_near, -1, own_rows, features)
             near_sum = summed(exchange(blocks, "near"))
-            hidden_out = summed(exchange(near_sum.astype(jnp.bfloat16), "far"))
+            hidden_out = summed(exchange(near_sum.astype(jnp.bfloat16), FAR))
         else:
             near_sum = summed(exchange(head_terms.reshape(n_near, -1, features), "near"))
-            far_sum = summed(copies(near_sum.astype(jnp.bfloat16), "far"))
+            far_sum = summed(copies(near_sum.astype(jnp.bfloat16), FAR))
             hidden = copies(far_sum.astype(jnp.bfloat16), "near").reshape(batch, features)
     return (hidden_out.astype(jnp.bfloat16), jnp.stack(states))
 
@@ -138,7 +142,9 @@
 def solution(mesh):
     sizes = mesh.shape
     fine = Mesh(
-        mesh.devices.reshape(sizes["grp"], sizes["tp"] // NEAR, NEAR, sizes["dp"]),
+        mesh.devices.reshape(
+            sizes["grp"], HALVES, sizes["tp"] // (HALVES * NEAR), NEAR, sizes["dp"]
+        ),
         ("grp", *TP, "dp"),
     )
 

time: 210 us -> 210 us (level)
  starting transfers between devices: 55.3 us -> 60.8 us
  blocking collectives: 85.9 us -> 80.5 us
    all_to_all x3, starting transfers between devices: 55.3 us -> 60.8 us  [exchange(): return lax.all_to_all(blocks, axes, split_axis=0, concat_axis=0, tiled=True)]
    all_to_all x7, blocking collectives: 85.9 us -> 80.5 us  [exchange(): return lax.all_to_all(blocks, axes, split_axis=0, concat_axis=0, tiled=True)]
where the time goes in v1:
time: 210 us; the launch traced here: 209 us
  blocking collectives  80.5 us (38%)
  starting transfers between devices  60.8 us (29%)
  waiting for transfers between devices  53.9 us (26%)
  local copies, waits for them, and re-layouts  6.75 us (3%)
  other arithmetic  5.11 us (2%)
    all_to_all x7, blocking collectives, exchange(): return lax.all_to_all(blocks, axes, split_axis=0, concat_axis=0, tiled=True)  80.5 us
    all_to_all x3, starting transfers between devices, exchange(): return lax.all_to_all(blocks, axes, split_axis=0, concat_axis=0, tiled=True)  60.8 us
    all_to_all x3, waiting for transfers between devices, exchange(): return lax.all_to_all(blocks, axes, split_axis=0, concat_axis=0, tiled=True)  53.9 us
  transfers between devices with their start and end apart: 3, of which 3 were waited for; matrix products, arithmetic and copies ran while one was open for 1% of the time, Pallas kernels for 0%

profile of v1, /device:TPU:40, one launch (start us, length us, event | category | flops | bytes accessed | tf_op | source)
XLA Modules:
  0.0 208.8 jit_solution(16674454673546244066)
XLA Ops:
  0.6 1.4 broadcast_in_dim.10
  2.0 45.9 %all-to-all-start = ((bf16[32,3,512]{2,1,0:T(4,128)(2,1)}), bf16[32,3,512]{2,1,0:T(4,128)(2,1)S(1)}, u32[]{:S(2)}, u32[]{:S(2)}) async-start(bf16[32,3,512]{2,1,0:T(4,128)(2,1)} %broadcast_in_dim.10), calls=%async_computation | async-start | bytes 262144 | tf_op jit(solution)/shard_map/all_to_all | solution.py:29
  48.0 0.9 copy-done.2
  49.0 0.9 copy-done.6
  50.6 0.3 concatenate.21
  51.0 0.3 concatenate.20
  51.4 0.3 copy-done.8
  51.7 27.1 %all-to-all-done = bf16[32,3,512]{2,1,0:T(4,128)(2,1)S(1)} async-done(((bf16[32,3,512]{2,1,0:T(4,128)(2,1)}), bf16[32,3,512]{2,1,0:T(4,128)(2,1)S(1)}, u32[]{:S(2)}, u32[]{:S(2)}) %all-to-all-start) | async-done | bytes 98336 | tf_op jit(solution)/shard_map/all_to_all | solution.py:29
  79.0 0.2 convolution_convert_fusion.1
  79.7 0.8 maximum_maximum_fusion
  80.4 4.7 %all-to-all-start.1 = ((bf16[8,12,512]{2,1,0:T(8,128)(2,1)}), bf16[8,12,512]{2,1,0:T(8,128)(2,1)S(1)}, u32[]{:S(2)}, u32[]{:S(2)}) async-start(bf16[8,12,512]{2,1,0:T(8,128)(2,1)} %maximum_maximum_fusion), calls=%async_computation.1 | async-start | bytes 262144 | tf_op jit(solution)/shard_map/all_to_all | solution.py:29
  85.2 6.1 %all-to-all-done.1 = bf16[8,12,512]{2,1,0:T(8,128)(2,1)S(1)} async-done(((bf16[8,12,512]{2,1,0:T(8,128)(2,1)}), bf16[8,12,512]{2,1,0:T(8,128)(2,1)S(1)}, u32[]{:S(2)}, u32[]{:S(2)}) %all-to-all-start.1) | async-done | bytes 98336 | tf_op jit(solution)/shard_map/all_to_all | solution.py:29
  91.3 0.2 slice_reduce_fusion.1
  91.6 0.4 fusion.7
  92.3 7.9 %all_to_all.50 = bf16[8,12,128]{2,1,0:T(8,128)(2,1)S(1)} all-to-all(bf16[8,12,128]{2,1,0:T(8,128)(2,1)S(1)} %broadcast_in_dim.11), channel_id=1, replica_groups=mesh['grp'=2,'half'=2,'stride'=4,'near'=4,'dp'=8] {'dp'}, dimensions={0} | all-to-all | bytes 49152 | tf_op jit(solution)/shard_map/all_to_all | solution.py:29
  100.2 0.2 fusion
  100.3 8.3 %all_to_all.51 = bf16[4,24,512]{2,1,0:T(8,128)(2,1)S(1)} all-to-all(bf16[4,24,512]{2,1,0:T(8,128)(2,1)S(1)} %bitcast.69), channel_id=1, replica_groups=mesh['grp'=2,'half'=2,'stride'=4,'near'=4,'dp'=8] {'near'}, dimensions={0} | all-to-all | bytes 196608 | tf_op jit(solution)/shard_map/all_to_all | solution.py:29
  108.6 28.4 %all_to_all.52 = bf16[8,24,512]{2,1,0:T(8,128)(2,1)S(1)} all-to-all(bf16[8,24,512]{2,1,0:T(8,128)(2,1)S(1)} %broadcast_in_dim.12), channel_id=1, replica_groups=mesh['grp'=2,'half'=2,'stride'=4,'near'=4,'dp'=8] {'stride','half'}, dimensions={0} | all-to-all | bytes 393216 | tf_op jit(solution)/shard_map/all_to_all | solution.py:29
  137.1 11.2 %all_to_all.53 = bf16[4,24,512]{2,1,0:T(8,128)(2,1)S(1)} all-to-all(bf16[4,24,512]{2,1,0:T(8,128)(2,1)S(1)} %broadcast_in_dim.13), channel_id=1, replica_groups=mesh['grp'=2,'half'=2,'stride'=4,'near'=4,'dp'=8] {'near'}, dimensions={0} | all-to-all | bytes 196608 | tf_op jit(solution)/shard_map/all_to_all | solution.py:29
  148.3 0.2 convolution_convert_fusion
  149.2 8.6 %all_to_all.54 = bf16[8,12,512]{2,1,0:T(8,128)(2,1)S(1)} all-to-all(bf16[8,12,512]{2,1,0:T(8,128)(2,1)S(1)} %maximum_maximum_fusion.1), channel_id=1, replica_groups=mesh['grp'=2,'half'=2,'stride'=4,'near'=4,'dp'=8] {'dp'}, dimensions={0} | all-to-all | bytes 196608 | tf_op jit(solution)/shard_map/all_to_all | solution.py:29
  157.8 0.2 slice_reduce_fusion
  158.1 0.4 fusion.4
  158.8 7.9 %all_to_all.55 = bf16[8,12,128]{2,1,0:T(8,128)(2,1)S(1)} all-to-all(bf16[8,12,128]{2,1,0:T(8,128)(2,1)S(1)} %broadcast_in_dim.14), channel_id=1, replica_groups=mesh['grp'=2,'half'=2,'stride'=4,'near'=4,'dp'=8] {'dp'}, dimensions={0} | all-to-all | bytes 49152 | tf_op jit(solution)/shard_map/all_to_all | solution.py:29
  166.6 0.2 fusion.1
  167.0 8.3 %all_to_all.56 = bf16[4,8,3,512]{3,1,2,0:T(8,128)(2,1)S(1)} all-to-all(bf16[4,8,3,512]{3,1,2,0:T(8,128)(2,1)S(1)} %copy.122), channel_id=1, replica_groups=mesh['grp'=2,'half'=2,'stride'=4,'near'=4,'dp'=8] {'near'}, dimensions={0} | all-to-all | bytes 196608 | tf_op jit(solution)/shard_map/all_to_all | solution.py:29
  175.2 0.6 copy.123
  175.9 10.2 %all-to-all-start.9 = ((bf16[8,3,512]{2,1,0:T(4,128)(2,1)}), bf16[8,3,512]{2,1,0:T(4,128)(2,1)S(1)}, u32[]{:S(2)}, u32[]{:S(2)}) async-start(bf16[8,3,512]{2,1,0:T(4,128)(2,1)} %copy.123), calls=%async_computation.9 | async-start | bytes 65536 | tf_op jit(solution)/shard_map/all_to_all | solution.py:29
  186.0 0.5 multiply_add_fusion.1
  186.5 0.9 pad_maximum_fusion
  187.4 20.7 %all-to-all-done.9 = bf16[8,3,512]{2,1,0:T(4,128)(2,1)S(1)} async-done(((bf16[8,3,512]{2,1,0:T(4,128)(2,1)}), bf16[8,3,512]{2,1,0:T(4,128)(2,1)S(1)}, u32[]{:S(2)}, u32[]{:S(2)}) %all-to-all-start.9) | async-done | bytes 24608 | tf_op jit(solution)/shard_map/all_to_all | solution.py:29
  208.2 0.6 reduce_sum.157
  (76 shorter events, 3.3 us)
Async XLA Ops:
  2.0 45.9 %copy-start.4 = (bf16[2,512,64]{1,2,0:T(8,128)(2,1)S(1)}, bf16[2,512,64]{1,2,0:T(8,128)(2,1)}, u32[]{:S(2)}) copy-start(bf16[2,512,64]{1,2,0:T(8,128)(2,1)} %param.15) | copy-start | bytes 393220
  2.0 46.0 %copy-start.5 = (bf16[2,512,64]{1,2,0:T(8,128)(2,1)S(1)}, bf16[2,512,64]{1,2,0:T(8,128)(2,1)}, u32[]{:S(2)}) copy-start(bf16[2,512,64]{1,2,0:T(8,128)(2,1)} %param.13) | copy-start | bytes 393220
  2.0 76.8 %all-to-all-start = ((bf16[32,3,512]{2,1,0:T(4,128)(2,1)}), bf16[32,3,512]{2,1,0:T(4,128)(2,1)S(1)}, u32[]{:S(2)}, u32[]{:S(2)}) async-start(bf16[32,3,512]{2,1,0:T(4,128)(2,1)} %broadcast_in_dim.10), calls=%async_computation | async-start | bytes 262144 | tf_op jit(solution)/shard_map/all_to_all | solution.py:29
  47.9 1.0 copy-start.2
  47.9 1.0 copy-start.3
  49.0 0.9 copy-start.6
  50.9 0.7 copy-start.8
  51.0 0.7 copy-start.7
  79.3 12.4 %copy-start = (f32[2,12,1,64,128]{4,3,2,1,0:T(8,128)S(1)}, f32[2,12,1,64,128]{4,3,2,1,0:T(8,128)}, u32[]{:S(2)}) copy-start(f32[2,12,1,64,128]{4,3,2,1,0:T(8,128)} %param.21) | copy-start | bytes 2359300
  80.4 4.7 %copy-start.9 = (f32[2,128]{1,0:T(2,128)S(1)}, f32[2,128]{1,0:T(2,128)}, u32[]{:S(2)}) copy-start(f32[2,128]{1,0:T(2,128)} %param.18) | copy-start | bytes 3076
  80.4 10.8 %all-to-all-start.1 = ((bf16[8,12,512]{2,1,0:T(8,128)(2,1)}), bf16[8,12,512]{2,1,0:T(8,128)(2,1)S(1)}, u32[]{:S(2)}, u32[]{:S(2)}) async-start(bf16[8,12,512]{2,1,0:T(8,128)(2,1)} %maximum_maximum_fusion), calls=%async_computation.1 | async-start | bytes 262144 | tf_op jit(solution)/shard_map/all_to_all | solution.py:29
  91.6 8.5 %copy-start.1 = (bf16[2,128,512]{2,1,0:T(8,128)(2,1)S(1)}, bf16[2,128,512]{2,1,0:T(8,128)(2,1)}, u32[]{:S(2)}) copy-start(bf16[2,128,512]{2,1,0:T(8,128)(2,1)} %param.19) | copy-start | bytes 786436
  175.9 32.3 %all-to-all-start.9 = ((bf16[8,3,512]{2,1,0:T(4,128)(2,1)}), bf16[8,3,512]{2,1,0:T(4,128)(2,1)S(1)}, u32[]{:S(2)}, u32[]{:S(2)}) async-start(bf16[8,3,512]{2,1,0:T(4,128)(2,1)} %copy.123), calls=%async_computation.9 | async-start | bytes 65536 | tf_op jit(solution)/shard_map/all_to_all | solution.py:29

commit v2 on v1

--- a/solution.py
+++ b/solution.py
@@ -17,8 +17,8 @@
 
 HALVES = 2
 
-TP = ("half", "stride", "near")
-FAR = ("stride", "half")
+TP = ("half", "quarter", "eighth", "near")
+FAR = ("quarter", "eighth", "half")
 
 
 def size_of(axes):
@@ -133,9 +133,10 @@
             near_sum = summed(exchange(blocks, "near"))
             hidden_out = summed(exchange(near_sum.astype(jnp.bfloat16), FAR))
         else:
-            near_sum = summed(exchange(head_terms.reshape(n_near, -1, features), "near"))
-            far_sum = summed(copies(near_sum.astype(jnp.bfloat16), FAR))
-            hidden = copies(far_sum.astype(jnp.bfloat16), "near").reshape(batch, features)
+            wide = ("eighth", "near")
+            near_sum = summed(exchange(head_terms.reshape(size_of(wide), -1, features), wide))
+            far_sum = summed(copies(near_sum.astype(jnp.bfloat16), ("quarter", "half")))
+            hidden = copies(far_sum.astype(jnp.bfloat16), wide).reshape(batch, features)
     return (hidden_out.astype(jnp.bfloat16), jnp.stack(states))
 
 
@@ -143,7 +144,7 @@
     sizes = mesh.shape
     fine = Mesh(
         mesh.devices.reshape(
-            sizes["grp"], HALVES, sizes["tp"] // (HALVES * NEAR), NEAR, sizes["dp"]
+            sizes["grp"], HALVES, sizes["tp"] // (2 * HALVES * NEAR), 2, NEAR, sizes["dp"]
         ),
         ("grp", *TP, "dp"),
     )

time: 210 us -> 216 us (1.029)
  blocking collectives: 80.5 us -> 93.5 us
  starting transfers between devices: 60.8 us -> 54.2 us
    all_to_all x7, blocking collectives: 80.5 us -> 93.5 us  [exchange(): return lax.all_to_all(blocks, axes, split_axis=0, concat_axis=0, tiled=True)]
    all_to_all x3, starting transfers between devices: 60.8 us -> 54.2 us  [exchange(): return lax.all_to_all(blocks, axes, split_axis=0, concat_axis=0, tiled=True)]
where the time goes in v2:
time: 216 us; the launch traced here: 215 us
  blocking collectives  93.5 us (43%)
  starting transfers between devices  54.2 us (25%)
  waiting for transfers between devices  53.6 us (25%)
  local copies, waits for them, and re-layouts  6.71 us (3%)
  other arithmetic  5.09 us (2%)
    all_to_all x7, blocking collectives, exchange(): return lax.all_to_all(blocks, axes, split_axis=0, concat_axis=0, tiled=True)  93.5 us
    all_to_all x3, starting transfers between devices, exchange(): return lax.all_to_all(blocks, axes, split_axis=0, concat_axis=0, tiled=True)  54.2 us
    all_to_all x3, waiting for transfers between devices, exchange(): return lax.all_to_all(blocks, axes, split_axis=0, concat_axis=0, tiled=True)  53.6 us
  transfers between devices with their start and end apart: 3, of which 3 were waited for; matrix products, arithmetic and copies ran while one was open for 1% of the time, Pallas kernels for 0%

profile of v2, /device:TPU:40, one launch (start us, length us, event | category | flops | bytes accessed | tf_op | source)
XLA Modules:
  0.0 214.9 jit_solution(5465058920280321568)
XLA Ops:
  0.6 1.4 broadcast_in_dim.10
  2.0 45.9 %all-to-all-start = ((bf16[32,3,512]{2,1,0:T(4,128)(2,1)}), bf16[32,3,512]{2,1,0:T(4,128)(2,1)S(1)}, u32[]{:S(2)}, u32[]{:S(2)}) async-start(bf16[32,3,512]{2,1,0:T(4,128)(2,1)} %broadcast_in_dim.10), calls=%async_computation | async-start | bytes 262144 | tf_op jit(solution)/shard_map/all_to_all | solution.py:29
  48.0 0.9 copy-done.2
  49.0 0.9 copy-done.6
  50.6 0.3 concatenate.21
  51.0 0.3 concatenate.20
  51.4 0.3 copy-done.8
  51.7 27.1 %all-to-all-done = bf16[32,3,512]{2,1,0:T(4,128)(2,1)S(1)} async-done(((bf16[32,3,512]{2,1,0:T(4,128)(2,1)}), bf16[32,3,512]{2,1,0:T(4,128)(2,1)S(1)}, u32[]{:S(2)}, u32[]{:S(2)}) %all-to-all-start) | async-done | bytes 98336 | tf_op jit(solution)/shard_map/all_to_all | solution.py:29
  79.0 0.2 convolution_convert_fusion.1
  79.7 0.8 maximum_maximum_fusion
  80.4 4.7 %all-to-all-start.1 = ((bf16[8,12,512]{2,1,0:T(8,128)(2,1)}), bf16[8,12,512]{2,1,0:T(8,128)(2,1)S(1)}, u32[]{:S(2)}, u32[]{:S(2)}) async-start(bf16[8,12,512]{2,1,0:T(8,128)(2,1)} %maximum_maximum_fusion), calls=%async_computation.1 | async-start | bytes 262144 | tf_op jit(solution)/shard_map/all_to_all | solution.py:29
  85.2 6.1 %all-to-all-done.1 = bf16[8,12,512]{2,1,0:T(8,128)(2,1)S(1)} async-done(((bf16[8,12,512]{2,1,0:T(8,128)(2,1)}), bf16[8,12,512]{2,1,0:T(8,128)(2,1)S(1)}, u32[]{:S(2)}, u32[]{:S(2)}) %all-to-all-start.1) | async-done | bytes 98336 | tf_op jit(solution)/shard_map/all_to_all | solution.py:29
  91.3 0.2 slice_reduce_fusion.1
  91.6 0.4 fusion.7
  92.3 7.9 %all_to_all.50 = bf16[8,12,128]{2,1,0:T(8,128)(2,1)S(1)} all-to-all(bf16[8,12,128]{2,1,0:T(8,128)(2,1)S(1)} %broadcast_in_dim.11), channel_id=1, replica_groups=mesh['grp'=2,'half'=2,'quarter'=2,'eighth'=2,'near'=4,'dp'=8] {'dp'}, dimensions={0} | all-to-all | bytes 49152 | tf_op jit(solution)/shard_map/all_to_all | solution.py:29
  100.2 0.2 fusion
  100.4 14.7 %all_to_all.51 = bf16[8,12,512]{2,1,0:T(8,128)(2,1)S(1)} all-to-all(bf16[8,12,512]{2,1,0:T(8,128)(2,1)S(1)} %reshape.278), channel_id=1, replica_groups=mesh['grp'=2,'half'=2,'quarter'=2,'eighth'=2,'near'=4,'dp'=8] {'eighth',..., dimensions={0} | all-to-all | bytes 196608 | tf_op jit(solution)/shard_map/all_to_all | solution.py:29
  115.1 30.2 %all_to_all.52 = bf16[4,12,512]{2,1,0:T(8,128)(2,1)S(1)} all-to-all(bf16[4,12,512]{2,1,0:T(8,128)(2,1)S(1)} %broadcast_in_dim.12), channel_id=1, replica_groups=mesh['grp'=2,'half'=2,'quarter'=2,'eighth'=2,'near'=4,'dp'=8] {'quarter'..., dimensions={0} | all-to-all | bytes 98304 | tf_op jit(solution)/shard_map/all_to_all | solution.py:29
  145.3 16.0 %all_to_all.53 = bf16[8,12,512]{2,1,0:T(8,128)(2,1)S(1)} all-to-all(bf16[8,12,512]{2,1,0:T(8,128)(2,1)S(1)} %broadcast_in_dim.13), channel_id=1, replica_groups=mesh['grp'=2,'half'=2,'quarter'=2,'eighth'=2,'near'=4,'dp'=8] {'eighth',..., dimensions={0} | all-to-all | bytes 196608 | tf_op jit(solution)/shard_map/all_to_all | solution.py:29
  161.4 0.2 convolution_convert_fusion
  162.2 8.6 %all_to_all.54 = bf16[8,12,512]{2,1,0:T(8,128)(2,1)S(1)} all-to-all(bf16[8,12,512]{2,1,0:T(8,128)(2,1)S(1)} %maximum_maximum_fusion.1), channel_id=1, replica_groups=mesh['grp'=2,'half'=2,'quarter'=2,'eighth'=2,'near'=4,'dp'=8] {'dp'}, dimensions={0} | all-to-all | bytes 196608 | tf_op jit(solution)/shard_map/all_to_all | solution.py:29
  170.8 0.2 slice_reduce_fusion
  171.1 0.4 fusion.4
  171.7 7.9 %all_to_all.55 = bf16[8,12,128]{2,1,0:T(8,128)(2,1)S(1)} all-to-all(bf16[8,12,128]{2,1,0:T(8,128)(2,1)S(1)} %broadcast_in_dim.14), channel_id=1, replica_groups=mesh['grp'=2,'half'=2,'quarter'=2,'eighth'=2,'near'=4,'dp'=8] {'dp'}, dimensions={0} | all-to-all | bytes 49152 | tf_op jit(solution)/shard_map/all_to_all | solution.py:29
  179.6 0.2 fusion.1
  179.9 8.3 %all_to_all.56 = bf16[4,8,3,512]{3,1,2,0:T(8,128)(2,1)S(1)} all-to-all(bf16[4,8,3,512]{3,1,2,0:T(8,128)(2,1)S(1)} %copy.139), channel_id=1, replica_groups=mesh['grp'=2,'half'=2,'quarter'=2,'eighth'=2,'near'=4,'dp'=8] {'near'}, dimensions={0} | all-to-all | bytes 196608 | tf_op jit(solution)/shard_map/all_to_all | solution.py:29
  188.2 0.6 copy.140
  188.8 3.5 %all-to-all-start.9 = ((bf16[8,3,512]{2,1,0:T(4,128)(2,1)}), bf16[8,3,512]{2,1,0:T(4,128)(2,1)S(1)}, u32[]{:S(2)}, u32[]{:S(2)}) async-start(bf16[8,3,512]{2,1,0:T(4,128)(2,1)} %copy.140), calls=%async_computation.9 | async-start | bytes 65536 | tf_op jit(solution)/shard_map/all_to_all | solution.py:29
  192.4 0.5 multiply_add_fusion.1
  192.9 0.9 pad_maximum_fusion
  193.8 20.4 %all-to-all-done.9 = bf16[8,3,512]{2,1,0:T(4,128)(2,1)S(1)} async-done(((bf16[8,3,512]{2,1,0:T(4,128)(2,1)}), bf16[8,3,512]{2,1,0:T(4,128)(2,1)S(1)}, u32[]{:S(2)}, u32[]{:S(2)}) %all-to-all-start.9) | async-done | bytes 24608 | tf_op jit(solution)/shard_map/all_to_all | solution.py:29
  214.2 0.6 reduce_sum.157
  (76 shorter events, 3.3 us)
Async XLA Ops:
  2.0 45.9 %copy-start.4 = (bf16[2,512,64]{1,2,0:T(8,128)(2,1)S(1)}, bf16[2,512,64]{1,2,0:T(8,128)(2,1)}, u32[]{:S(2)}) copy-start(bf16[2,512,64]{1,2,0:T(8,128)(2,1)} %param.15) | copy-start | bytes 393220
  2.0 46.0 %copy-start.5 = (bf16[2,512,64]{1,2,0:T(8,128)(2,1)S(1)}, bf16[2,512,64]{1,2,0:T(8,128)(2,1)}, u32[]{:S(2)}) copy-start(bf16[2,512,64]{1,2,0:T(8,128)(2,1)} %param.13) | copy-start | bytes 393220
  2.0 76.8 %all-to-all-start = ((bf16[32,3,512]{2,1,0:T(4,128)(2,1)}), bf16[32,3,512]{2,1,0:T(4,128)(2,1)S(1)}, u32[]{:S(2)}, u32[]{:S(2)}) async-start(bf16[32,3,512]{2,1,0:T(4,128)(2,1)} %broadcast_in_dim.10), calls=%async_computation | async-start | bytes 262144 | tf_op jit(solution)/shard_map/all_to_all | solution.py:29
  47.9 1.0 copy-start.2
  47.9 1.0 copy-start.3
  49.0 0.9 copy-start.6
  50.9 0.7 copy-start.8
  51.0 0.7 copy-start.7
  79.3 12.4 %copy-start = (f32[2,12,1,64,128]{4,3,2,1,0:T(8,128)S(1)}, f32[2,12,1,64,128]{4,3,2,1,0:T(8,128)}, u32[]{:S(2)}) copy-start(f32[2,12,1,64,128]{4,3,2,1,0:T(8,128)} %param.21) | copy-start | bytes 2359300
  80.4 4.7 %copy-start.9 = (f32[2,128]{1,0:T(2,128)S(1)}, f32[2,128]{1,0:T(2,128)}, u32[]{:S(2)}) copy-start(f32[2,128]{1,0:T(2,128)} %param.18) | copy-start | bytes 3076
  80.4 10.8 %all-to-all-start.1 = ((bf16[8,12,512]{2,1,0:T(8,128)(2,1)}), bf16[8,12,512]{2,1,0:T(8,128)(2,1)S(1)}, u32[]{:S(2)}, u32[]{:S(2)}) async-start(bf16[8,12,512]{2,1,0:T(8,128)(2,1)} %maximum_maximum_fusion), calls=%async_computation.1 | async-start | bytes 262144 | tf_op jit(solution)/shard_map/all_to_all | solution.py:29
  91.6 8.5 %copy-start.1 = (bf16[2,128,512]{2,1,0:T(8,128)(2,1)S(1)}, bf16[2,128,512]{2,1,0:T(8,128)(2,1)}, u32[]{:S(2)}) copy-start(bf16[2,128,512]{2,1,0:T(8,128)(2,1)} %param.19) | copy-start | bytes 786436
  188.8 25.4 %all-to-all-start.9 = ((bf16[8,3,512]{2,1,0:T(4,128)(2,1)}), bf16[8,3,512]{2,1,0:T(4,128)(2,1)S(1)}, u32[]{:S(2)}, u32[]{:S(2)}) async-start(bf16[8,3,512]{2,1,0:T(4,128)(2,1)} %copy.140), calls=%async_computation.9 | async-start | bytes 65536 | tf_op jit(solution)/shard_map/all_to_all | solution.py:29

commit v3 on v2

--- a/solution.py
+++ b/solution.py
@@ -62,7 +62,9 @@
     own_rows, features = hidden_in.shape
     n_dp = size_of("dp")
     n_near = size_of("near")
-    hidden = lax.optimization_barrier(copies(hidden_in, TP).reshape(-1, features))
+    hidden = copies(hidden_in, ("half", "quarter", "eighth"))
+    hidden = copies(hidden, "near").swapaxes(0, 1).reshape(-1, features)
+    hidden = lax.optimization_barrier(hidden)
     joined = lax.optimization_barrier(
         [
             jnp.concatenate(
@@ -133,10 +135,9 @@
             near_sum = summed(exchange(blocks, "near"))
             hidden_out = summed(exchange(near_sum.astype(jnp.bfloat16), FAR))
         else:
-            wide = ("eighth", "near")
-            near_sum = summed(exchange(head_terms.reshape(size_of(wide), -1, features), wide))
-            far_sum = summed(copies(near_sum.astype(jnp.bfloat16), ("quarter", "half")))
-            hidden = copies(far_sum.astype(jnp.bfloat16), wide).reshape(batch, features)
+            near_sum = summed(exchange(head_terms.reshape(n_near, -1, features), "near"))
+            far_sum = summed(copies(near_sum.astype(jnp.bfloat16), ("half", "eighth", "quarter")))
+            hidden = copies(far_sum.astype(jnp.bfloat16), "near").reshape(batch, features)
     return (hidden_out.astype(jnp.bfloat16), jnp.stack(states))
 
 

time: 216 us -> 212 us (0.981)
  blocking collectives: 93.5 us -> 86.4 us
  starting transfers between devices: 54.2 us -> 58.3 us
  waiting for transfers between devices: 53.6 us -> 51.3 us
    all_to_all x7, blocking collectives: 93.5 us -> 86.4 us  [exchange(): return lax.all_to_all(blocks, axes, split_axis=0, concat_axis=0, tiled=True)]
    all_to_all x3 -> x4, starting transfers between devices: 54.2 us -> 58.3 us  [exchange(): return lax.all_to_all(blocks, axes, split_axis=0, concat_axis=0, tiled=True)]
    all_to_all x3 -> x4, waiting for transfers between devices: 53.6 us -> 51.3 us  [exchange(): return lax.all_to_all(blocks, axes, split_axis=0, concat_axis=0, tiled=True)]
  transfers between devices with their start and end apart: 3 -> 4, of which waited for: 3 -> 4; matrix products, arithmetic and copies ran while one was open for 1% -> 2% of each run, Pallas kernels for 0% -> 0%
where the time goes in v3:
time: 212 us; the launch traced here: 211 us
  blocking collectives  86.4 us (41%)
  starting transfers between devices  58.3 us (28%)
  waiting for transfers between devices  51.3 us (24%)
  local copies, waits for them, and re-layouts  8.3 us (4%)
  other arithmetic  5.11 us (2%)
    all_to_all x7, blocking collectives, exchange(): return lax.all_to_all(blocks, axes, split_axis=0, concat_axis=0, tiled=True)  86.4 us
    all_to_all x4, starting transfers between devices, exchange(): return lax.all_to_all(blocks, axes, split_axis=0, concat_axis=0, tiled=True)  58.3 us
    all_to_all x4, waiting for transfers between devices, exchange(): return lax.all_to_all(blocks, axes, split_axis=0, concat_axis=0, tiled=True)  51.3 us
  transfers between devices with their start and end apart: 4, of which 4 were waited for; matrix products, arithmetic and copies ran while one was open for 2% of the time, Pallas kernels for 0%

profile of v3, /device:TPU:40, one launch (start us, length us, event | category | flops | bytes accessed | tf_op | source)
XLA Modules:
  0.0 211.1 jit_solution(12587558109474957455)
XLA Ops:
  0.6 1.3 broadcast_in_dim.12
  1.9 43.4 %all-to-all-start = ((bf16[8,3,512]{2,1,0:T(4,128)(2,1)}), bf16[8,3,512]{2,1,0:T(4,128)(2,1)S(1)}, u32[]{:S(2)}, u32[]{:S(2)}) async-start(bf16[8,3,512]{2,1,0:T(4,128)(2,1)} %broadcast_in_dim.12), calls=%async_computation | async-start | bytes 65536 | tf_op jit(solution)/shard_map/all_to_all | solution.py:29
  45.4 0.9 fusion.29
  46.4 0.8 copy-done.4
  47.3 0.8 copy-done.5
  48.6 0.6 copy-done.2
  49.3 0.3 concatenate.21
  49.6 0.3 concatenate.20
  50.0 18.7 %all-to-all-done = bf16[8,3,512]{2,1,0:T(4,128)(2,1)S(1)} async-done(((bf16[8,3,512]{2,1,0:T(4,128)(2,1)}), bf16[8,3,512]{2,1,0:T(4,128)(2,1)S(1)}, u32[]{:S(2)}, u32[]{:S(2)}) %all-to-all-start) | async-done | bytes 24608 | tf_op jit(solution)/shard_map/all_to_all | solution.py:29
  68.7 0.6 broadcast_in_dim.13
  69.3 5.2 %all-to-all-start.1 = ((bf16[4,8,3,512]{3,1,2,0:T(8,128)(2,1)}), bf16[4,8,3,512]{3,1,2,0:T(8,128)(2,1)S(1)}, u32[]{:S(2)}, u32[]{:S(2)}) async-start(bf16[4,8,3,512]{3,1,2,0:T(8,128)(2,1)} %broadcast_in_dim.13), calls=%async_computation.1 | async-start | bytes 196608 | tf_op jit(solution)/shard_map/all_to_all | solution.py:29
  74.6 5.8 %all-to-all-done.1 = bf16[4,8,3,512]{3,1,2,0:T(8,128)(2,1)S(1)} async-done(((bf16[4,8,3,512]{3,1,2,0:T(8,128)(2,1)}), bf16[4,8,3,512]{3,1,2,0:T(8,128)(2,1)S(1)}, u32[]{:S(2)}, u32[]{:S(2)}) %all-to-all-start.1) | async-done | bytes 98336 | tf_op jit(solution)/shard_map/all_to_all | solution.py:29
  80.6 0.2 convolution_convert_fusion.1
  81.3 0.8 maximum_maximum_fusion
  82.0 4.7 %all-to-all-start.2 = ((bf16[8,12,512]{2,1,0:T(8,128)(2,1)}), bf16[8,12,512]{2,1,0:T(8,128)(2,1)S(1)}, u32[]{:S(2)}, u32[]{:S(2)}) async-start(bf16[8,12,512]{2,1,0:T(8,128)(2,1)} %maximum_maximum_fusion), calls=%async_computation.2 | async-start | bytes 262144 | tf_op jit(solution)/shard_map/all_to_all | solution.py:29
  86.8 6.1 %all-to-all-done.2 = bf16[8,12,512]{2,1,0:T(8,128)(2,1)S(1)} async-done(((bf16[8,12,512]{2,1,0:T(8,128)(2,1)}), bf16[8,12,512]{2,1,0:T(8,128)(2,1)S(1)}, u32[]{:S(2)}, u32[]{:S(2)}) %all-to-all-start.2) | async-done | bytes 98336 | tf_op jit(solution)/shard_map/all_to_all | solution.py:29
  93.2 0.4 fusion.7
  93.8 7.9 %all_to_all.55 = bf16[8,12,128]{2,1,0:T(8,128)(2,1)S(1)} all-to-all(bf16[8,12,128]{2,1,0:T(8,128)(2,1)S(1)} %broadcast_in_dim.14), channel_id=1, replica_groups=mesh['grp'=2,'half'=2,'quarter'=2,'eighth'=2,'near'=4,'dp'=8] {'dp'}, dimensions={0} | all-to-all | bytes 49152 | tf_op jit(solution)/shard_map/all_to_all | solution.py:29
  101.9 8.3 %all_to_all.56 = bf16[4,24,512]{2,1,0:T(8,128)(2,1)S(1)} all-to-all(bf16[4,24,512]{2,1,0:T(8,128)(2,1)S(1)} %bitcast.71), channel_id=1, replica_groups=mesh['grp'=2,'half'=2,'quarter'=2,'eighth'=2,'near'=4,'dp'=8] {'near'}, dimensions={0} | all-to-all | bytes 196608 | tf_op jit(solution)/shard_map/all_to_all | solution.py:29
  110.2 34.5 %all_to_all.57 = bf16[8,24,512]{2,1,0:T(8,128)(2,1)S(1)} all-to-all(bf16[8,24,512]{2,1,0:T(8,128)(2,1)S(1)} %broadcast_in_dim.15), channel_id=1, replica_groups=mesh['grp'=2,'half'=2,'quarter'=2,'eighth'=2,'near'=4,'dp'=8] {'half','e..., dimensions={0} | all-to-all | bytes 393216 | tf_op jit(solution)/shard_map/all_to_all | solution.py:29
  144.8 11.0 %all_to_all.58 = bf16[4,24,512]{2,1,0:T(8,128)(2,1)S(1)} all-to-all(bf16[4,24,512]{2,1,0:T(8,128)(2,1)S(1)} %broadcast_in_dim.16), channel_id=1, replica_groups=mesh['grp'=2,'half'=2,'quarter'=2,'eighth'=2,'near'=4,'dp'=8] {'near'}, dimensions={0} | all-to-all | bytes 196608 | tf_op jit(solution)/shard_map/all_to_all | solution.py:29
  155.8 0.2 convolution_convert_fusion
  156.7 8.6 %all_to_all.59 = bf16[8,12,512]{2,1,0:T(8,128)(2,1)S(1)} all-to-all(bf16[8,12,512]{2,1,0:T(8,128)(2,1)S(1)} %maximum_maximum_fusion.1), channel_id=1, replica_groups=mesh['grp'=2,'half'=2,'quarter'=2,'eighth'=2,'near'=4,'dp'=8] {'dp'}, dimensions={0} | all-to-all | bytes 196608 | tf_op jit(solution)/shard_map/all_to_all | solution.py:29
  165.6 0.4 fusion.4
  166.3 7.9 %all_to_all.60 = bf16[8,12,128]{2,1,0:T(8,128)(2,1)S(1)} all-to-all(bf16[8,12,128]{2,1,0:T(8,128)(2,1)S(1)} %broadcast_in_dim.17), channel_id=1, replica_groups=mesh['grp'=2,'half'=2,'quarter'=2,'eighth'=2,'near'=4,'dp'=8] {'dp'}, dimensions={0} | all-to-all | bytes 49152 | tf_op jit(solution)/shard_map/all_to_all | solution.py:29
  174.5 8.3 %all_to_all.61 = bf16[4,8,3,512]{3,1,2,0:T(8,128)(2,1)S(1)} all-to-all(bf16[4,8,3,512]{3,1,2,0:T(8,128)(2,1)S(1)} %copy.133), channel_id=1, replica_groups=mesh['grp'=2,'half'=2,'quarter'=2,'eighth'=2,'near'=4,'dp'=8] {'near'}, dimensions={0} | all-to-all | bytes 196608 | tf_op jit(solution)/shard_map/all_to_all | solution.py:29
  182.7 0.6 copy.134
  183.4 5.0 %all-to-all-start.10 = ((bf16[8,3,512]{2,1,0:T(4,128)(2,1)}), bf16[8,3,512]{2,1,0:T(4,128)(2,1)S(1)}, u32[]{:S(2)}, u32[]{:S(2)}) async-start(bf16[8,3,512]{2,1,0:T(4,128)(2,1)} %copy.134), calls=%async_computation.10 | async-start | bytes 65536 | tf_op jit(solution)/shard_map/all_to_all | solution.py:29
  188.4 0.5 multiply_add_fusion.1
  188.8 0.9 pad_maximum_fusion
  189.8 20.7 %all-to-all-done.10 = bf16[8,3,512]{2,1,0:T(4,128)(2,1)S(1)} async-done(((bf16[8,3,512]{2,1,0:T(4,128)(2,1)}), bf16[8,3,512]{2,1,0:T(4,128)(2,1)S(1)}, u32[]{:S(2)}, u32[]{:S(2)}) %all-to-all-start.10) | async-done | bytes 24608 | tf_op jit(solution)/shard_map/all_to_all | solution.py:29
  210.5 0.6 reduce_sum.157
  (79 shorter events, 4.0 us)
Async XLA Ops:
  1.9 66.7 %all-to-all-start = ((bf16[8,3,512]{2,1,0:T(4,128)(2,1)}), bf16[8,3,512]{2,1,0:T(4,128)(2,1)S(1)}, u32[]{:S(2)}, u32[]{:S(2)}) async-start(bf16[8,3,512]{2,1,0:T(4,128)(2,1)} %broadcast_in_dim.12), calls=%async_computation | async-start | bytes 65536 | tf_op jit(solution)/shard_map/all_to_all | solution.py:29
  46.3 0.9 copy-start.4
  47.2 0.9 copy-start.5
  48.2 1.0 copy-start.2
  48.2 1.0 copy-start.3
  69.3 5.2 %copy-start.7 = (f32[2,512]{1,0:T(2,128)S(1)}, f32[2,512]{1,0:T(2,128)}, u32[]{:S(2)}) copy-start(f32[2,512]{1,0:T(2,128)} %param.12) | copy-start | bytes 12292
  69.3 5.2 %copy-start.6 = (f32[2,12,64]{2,0,1:T(2,128)S(1)}, f32[2,12,64]{2,0,1:T(2,128)}, u32[]{:S(2)}) copy-start(f32[2,12,64]{2,0,1:T(2,128)} %param.20) | copy-start | bytes 18436
  69.3 11.0 %all-to-all-start.1 = ((bf16[4,8,3,512]{3,1,2,0:T(8,128)(2,1)}), bf16[4,8,3,512]{3,1,2,0:T(8,128)(2,1)S(1)}, u32[]{:S(2)}, u32[]{:S(2)}) async-start(bf16[4,8,3,512]{3,1,2,0:T(8,128)(2,1)} %broadcast_in_dim.13), calls=%async_computation.1 | async-start | bytes 196608 | tf_op jit(solution)/shard_map/all_to_all | solution.py:29
  80.8 12.4 %copy-start = (f32[2,12,1,64,128]{4,3,2,1,0:T(8,128)S(1)}, f32[2,12,1,64,128]{4,3,2,1,0:T(8,128)}, u32[]{:S(2)}) copy-start(f32[2,12,1,64,128]{4,3,2,1,0:T(8,128)} %param.21) | copy-start | bytes 2359300
  82.0 4.7 %copy-start.8 = (f32[2,128]{1,0:T(2,128)S(1)}, f32[2,128]{1,0:T(2,128)}, u32[]{:S(2)}) copy-start(f32[2,128]{1,0:T(2,128)} %param.18) | copy-start | bytes 3076
  82.0 10.8 %all-to-all-start.2 = ((bf16[8,12,512]{2,1,0:T(8,128)(2,1)}), bf16[8,12,512]{2,1,0:T(8,128)(2,1)S(1)}, u32[]{:S(2)}, u32[]{:S(2)}) async-start(bf16[8,12,512]{2,1,0:T(8,128)(2,1)} %maximum_maximum_fusion), calls=%async_computation.2 | async-start | bytes 262144 | tf_op jit(solution)/shard_map/all_to_all | solution.py:29
  93.2 8.5 %copy-start.1 = (bf16[2,128,512]{2,1,0:T(8,128)(2,1)S(1)}, bf16[2,128,512]{2,1,0:T(8,128)(2,1)}, u32[]{:S(2)}) copy-start(bf16[2,128,512]{2,1,0:T(8,128)(2,1)} %param.19) | copy-start | bytes 786436
  183.4 27.1 %all-to-all-start.10 = ((bf16[8,3,512]{2,1,0:T(4,128)(2,1)}), bf16[8,3,512]{2,1,0:T(4,128)(2,1)S(1)}, u32[]{:S(2)}, u32[]{:S(2)}) async-start(bf16[8,3,512]{2,1,0:T(4,128)(2,1)} %copy.134), calls=%async_computation.10 | async-start | bytes 65536 | tf_op jit(solution)/shard_map/all_to_all | solution.py:29
